TPU v7x, 32 devices: a whole 2x2x4 slice. The times are simulated.
32 devices in a mesh: sp: 16 (over z, y, core), tp: 2 (over x).
Axes of the slice: x: 2, y: 2, z: 4, core: 2. Of those that a mesh axis runs over, the one named last changes fastest.
Arguments:
- tokens_in: bfloat16 [4096, 2048], P('sp', 'tp'), may hold values from -400 to 400
- norm_gain: float32 [2048], replicated, may hold values from 0.1 to 1.9
- w_query: bfloat16 [2048, 1024], P('sp', 'tp'), may hold values from -0.125 to 0.125
- w_forget: bfloat16 [2048, 1024], P('sp', 'tp'), may hold values from -0.125 to 0.125
- w_input: bfloat16 [2048, 1024], P('sp', 'tp'), may hold values from -0.125 to 0.125
- w_rgate: bfloat16 [2048, 1024], P('sp', 'tp'), may hold values from -0.125 to 0.125
- w_pool_in: bfloat16 [2048, 1024], P('sp', 'tp'), may hold values from -0.125 to 0.125
- w_pgate: bfloat16 [2048, 1024], P('sp', 'tp'), may hold values from -0.125 to 0.125
- floor_rate: float32 [1024], P('tp'), as said below
- extra_logdecay: float32 [4096, 8], P('sp', 'tp'), as said below
- state_gain: float32 [1024], P('tp'), may hold values from 0.1 to 1.9
- pool_mix: bfloat16 [8, 128, 128], P('tp'), may hold values from -0.5 to 0.5
- pool_gain: float32 [1024], P('tp'), may hold values from 0.1 to 1.9
- out_rec: bfloat16 [1024, 2048], P('tp', 'sp'), may hold values from -0.125 to 0.125
- out_pool: bfloat16 [1024, 2048], P('tp', 'sp'), may hold values from -0.125 to 0.125
- post_gain: float32 [2048], replicated, may hold values from 0.1 to 1.9
Outputs:
- mixed_out: bfloat16 [4096, 2048], P(('sp', 'tp'))
Inputs may be any that keep to these rules, and one draw needn't show every extreme that they name: `floor_rate`: every entry is positive. `extra_logdecay`: every entry is at most zero.
All inputs are finite; a program needn't handle non-finite values.
Results may differ from a plain program's by a relative error of at most 0.015.
Values may be sent and summed in bfloat16 or wider, within the bound.
A program may use at most 64 MiB of HBM per device.

v0:
```python
import jax
import jax.numpy as jnp
from jax import lax
from jax.sharding import PartitionSpec as P

DK = 128
BLOCK = 64
eps = 1e-06
coarsest_scale_depth = lax.Precision.HIGHEST


def prefix(part, axis, combine, identity):
    place = lax.axis_index(axis)
    gathered = jax.tree.map(lambda a: lax.all_gather(a, axis), part)
    state = jax.tree.map(lambda a, e: jnp.zeros_like(a) + jnp.asarray(e, a.dtype), part, identity)

    def one(turn, state):
        return combine(
            state, jax.tree.map(lambda a: lax.dynamic_index_in_dim(a, turn, 0, False), gathered)
        )

    return lax.fori_loop(0, place, one, state)


def shifted(value, axis, steps):
    count = lax.axis_size(axis)
    initial, last = (max(0, -steps), min(count, count - steps))
    return lax.ppermute(value, axis, [(source, source + steps) for source in range(initial, last)])


def chain_merge(earlier, later):
    return (earlier[0] * later[0], later[0][..., None] * earlier[1] + later[1])


def local_blocks(qs, keys, values, logs):
    causal = jnp.arange(BLOCK)[:, None] >= jnp.arange(BLOCK)[None, :]
    heads_dev = qs.shape[1]

    def advance(carry, member):
        carried_memory_matrix, start = carry
        probe_segment, key_piece, input_piece, gc = member
        prefix_sum_vector = jnp.cumsum(gc, axis=1)
        last_index = prefix_sum_vector[:, -1]
        cross_segment_contribution = jnp.einsum(
            "abz,azy->aby",
            probe_segment * jnp.exp(prefix_sum_vector),
            carried_memory_matrix,
            precision=coarsest_scale_depth,
        )
        diff = prefix_sum_vector[:, :, None, :] - prefix_sum_vector[:, None, :, :]
        weight = jnp.where(causal[None, :, :, None], jnp.exp(jnp.minimum(diff, 0.0)), 0.0)
        scores = jnp.einsum(
            "htk,hsk,htsk->hts", probe_segment, key_piece, weight, precision=coarsest_scale_depth
        )
        final_result = cross_segment_contribution + jnp.einsum(
            "hts,hsv->htv", scores, input_piece, precision=coarsest_scale_depth
        )
        carried_memory_matrix = jnp.exp(last_index)[..., None] * carried_memory_matrix + jnp.einsum(
            "njp,njq->npq",
            key_piece * jnp.exp(last_index[:, None, :] - prefix_sum_vector),
            input_piece,
            precision=coarsest_scale_depth,
        )
        pool_reach = probe_segment * jnp.exp(start[:, None, :] + prefix_sum_vector)
        return ((carried_memory_matrix, start + last_index), (final_result, pool_reach))

    begin = (jnp.zeros((heads_dev, DK, DK), jnp.float32), jnp.zeros((heads_dev, DK), jnp.float32))
    (carried_memory_matrix, total), (final_result, pool_reach) = lax.scan(
        advance, begin, (qs, keys, values, logs)
    )
    return (carried_memory_matrix, total, final_result, pool_reach)


def per_device(
    tokens_in,
    norm_gain,
    w_query,
    w_forget,
    w_input,
    w_rgate,
    w_pool_in,
    w_pgate,
    floor_rate,
    extra_logdecay,
    state_gain,
    pool_mix,
    pool_gain,
    out_rec,
    out_pool,
    post_gain,
):
    gathered = (
        lax.all_gather(w_query, "sp", axis=0, tiled=True),
        lax.all_gather(w_forget, "sp", axis=0, tiled=True),
        lax.all_gather(w_input, "sp", axis=0, tiled=True),
        lax.all_gather(w_rgate, "sp", axis=0, tiled=True),
        lax.all_gather(w_pool_in, "sp", axis=0, tiled=True),
        lax.all_gather(w_pgate, "sp", axis=0, tiled=True),
    )
    joined = jnp.concatenate(gathered, axis=1)
    head_cols = w_query.shape[1]
    positions = tokens_in.shape[0]
    model_width = norm_gain.shape[0]
    wide = lax.all_gather(tokens_in, "tp", axis=1, tiled=True).astype(jnp.float32)
    scaled = (wide * norm_gain[None, :]).astype(jnp.bfloat16)
    totals = jnp.dot(scaled, joined, preferred_element_type=jnp.float32)
    squares = jnp.sum(wide * wide, axis=1)
    inv_rms = lax.rsqrt(squares / model_width + eps)
    proj = (totals * inv_rms[:, None]).astype(jnp.bfloat16)
    query = proj[:, 0:head_cols]
    forget = proj[:, head_cols : 2 * head_cols]
    inputs = proj[:, 2 * head_cols : 3 * head_cols]
    rgate = proj[:, 3 * head_cols : 4 * head_cols]
    pool_in = proj[:, 4 * head_cols : 5 * head_cols]
    pgate = proj[:, 5 * head_cols : 6 * head_cols]
    heads_dev = head_cols // DK
    blocks = positions // BLOCK

    def to_blocks(array):
        return array.reshape(blocks, BLOCK, heads_dev, DK).transpose(0, 2, 1, 3)

    forget32 = forget.astype(jnp.float32)
    key_gate = -jnp.expm1(-floor_rate)[None, :] * jax.nn.sigmoid(-forget32)
    log_forget = jnp.log1p(-key_gate) + jnp.repeat(extra_logdecay, DK, axis=1)
    qs = query.astype(jnp.float32) * DK ** (-0.5)
    carried_memory_matrix, total, final_result, pool_reach = local_blocks(
        to_blocks(qs),
        to_blocks(key_gate),
        to_blocks(inputs.astype(jnp.float32)),
        to_blocks(log_forget),
    )
    decays = jnp.exp(total)
    tail_rows = pool_in[positions - 16 :]
    carried = prefix(
        (decays, carried_memory_matrix),
        "sp",
        chain_merge,
        (jnp.ones_like(decays), jnp.zeros_like(carried_memory_matrix)),
    )
    incoming_state = carried[1]
    previous = shifted(tail_rows, "sp", 1).astype(jnp.float32)
    recurrent_output = final_result + jnp.einsum(
        "izaf,zfu->izau", pool_reach, incoming_state, precision=coarsest_scale_depth
    )
    grouped = recurrent_output.transpose(0, 2, 1, 3).reshape(positions, heads_dev, DK)
    normed = grouped * lax.rsqrt(jnp.mean(grouped * grouped, axis=2, keepdims=True) + eps)
    y_rec = (
        normed.reshape(positions, head_cols)
        * state_gain[None, :]
        * jax.nn.silu(rgate.astype(jnp.float32))
    ).astype(jnp.bfloat16)
    group = lax.axis_index("tp") * heads_dev + jnp.arange(head_cols) // DK
    window = jnp.power(2, 1 + group % 4).astype(jnp.int32)
    pool32 = pool_in.astype(jnp.float32)
    extended = jnp.concatenate([previous, pool32], axis=0)
    summed_rows = jnp.zeros((positions, head_cols), jnp.float32)
    for offset in range(16):
        rows_back = extended[16 - offset : 16 - offset + positions]
        summed_rows = summed_rows + jnp.where((offset < window)[None, :], rows_back, 0.0)
    place = lax.axis_index("sp") * positions + jnp.arange(positions)
    count = jnp.minimum(place[:, None] + 1, window[None, :]).astype(jnp.float32)
    mixed = (summed_rows / count - pool32).astype(jnp.bfloat16)
    mapped = jnp.einsum(
        "tgc,gcd->tgd",
        mixed.reshape(positions, heads_dev, DK),
        pool_mix,
        preferred_element_type=jnp.float32,
    ).reshape(positions, head_cols)
    y_pool = (mapped * pool_gain[None, :] * jax.nn.silu(pgate.astype(jnp.float32))).astype(
        jnp.bfloat16
    )
    out_parts = (
        lax.all_gather(out_rec, "sp", axis=1, tiled=True),
        lax.all_gather(out_pool, "sp", axis=1, tiled=True),
    )
    both = jnp.concatenate([y_rec, y_pool], axis=1)
    weight_cat = jnp.concatenate(out_parts, axis=0)
    summed = lax.psum_scatter(
        jnp.dot(both, weight_cat, preferred_element_type=jnp.float32).astype(jnp.bfloat16),
        "tp",
        scatter_dimension=0,
        tiled=True,
    ).astype(jnp.float32)
    final = (
        summed
        * lax.rsqrt(jnp.mean(summed * summed, axis=1, keepdims=True) + eps)
        * post_gain[None, :]
    )
    return final.astype(jnp.bfloat16)


def solution(mesh):
    placed = (
        P("sp", "tp"),
        P(),
        P("sp", "tp"),
        P("sp", "tp"),
        P("sp", "tp"),
        P("sp", "tp"),
        P("sp", "tp"),
        P("sp", "tp"),
        P("tp"),
        P("sp", "tp"),
        P("tp"),
        P("tp", None, None),
        P("tp"),
        P("tp", "sp"),
        P("tp", "sp"),
        P(),
    )
    return jax.shard_map(
        per_device, mesh=mesh, in_specs=placed, out_specs=P(("sp", "tp"), None), check_vma=False
    )
```

profile of v0, /device:TPU:0, one launch (start us, length us, event | category | flops | bytes accessed | tf_op | source)
XLA Modules:
  0.0 518.1 jit_solution(14276728240443677830)
XLA Ops:
  6.5 0.7 all-gather.14.cloned.1.call-update
  7.3 0.7 all-gather.16.cloned.1.call-update
  8.1 0.7 all-gather.18.cloned.1.call-update
  8.8 0.5 all-gather.20.cloned.1.call-update
  9.4 0.5 all-gather.22.cloned.1.call-update
  10.0 0.5 all-gather.24.cloned.1.call-update
  10.5 0.7 all-gather.26.cloned.1.call-update
  11.3 0.8 copy.44
  12.1 0.7 exponential-minus-one_negate_fusion
  12.8 20.1 %all-gather.14.cloned.1.call-done = bf16[256,2048]{1,0:T(8,128)(2,1)} async-done(((bf16[256,1024]{1,0:T(8,128)(2,1)}), bf16[256,2048]{1,0:T(8,128)(2,1)}) %all-gather.14.cloned.1.call-update) | async-done | bytes 1048592 | tf_op jit(solution)/shard_map/all_gather | solution.py:104
  32.9 1.5 fusion.34
  34.4 42.1 %all-gather.16.cloned.1.call-done = bf16[2048,512]{1,0:T(8,128)(2,1)} async-done(((bf16[128,512]{1,0:T(8,128)(2,1)}), bf16[2048,512]{1,0:T(8,128)(2,1)}) %all-gather.16.cloned.1.call-update) | async-done | bytes 2097168 | tf_op jit(solution)/shard_map/all_gather | solution.py:93
  76.6 3.2 constant_dynamic-update-slice_fusion.5
  79.7 39.2 %all-gather.18.cloned.1.call-done = bf16[2048,512]{1,0:T(8,128)(2,1)} async-done(((bf16[128,512]{1,0:T(8,128)(2,1)}), bf16[2048,512]{1,0:T(8,128)(2,1)}) %all-gather.18.cloned.1.call-update) | async-done | bytes 2097168 | tf_op jit(solution)/shard_map/all_gather | solution.py:94
  118.9 3.2 constant_dynamic-update-slice_fusion.4
  122.2 39.0 %all-gather.20.cloned.1.call-done = bf16[2048,512]{1,0:T(8,128)(2,1)} async-done(((bf16[128,512]{1,0:T(8,128)(2,1)}), bf16[2048,512]{1,0:T(8,128)(2,1)}) %all-gather.20.cloned.1.call-update) | async-done | bytes 2097168 | tf_op jit(solution)/shard_map/all_gather | solution.py:95
  161.2 3.1 constant_dynamic-update-slice_fusion.3
  164.3 39.1 %all-gather.22.cloned.1.call-done = bf16[2048,512]{1,0:T(8,128)(2,1)} async-done(((bf16[128,512]{1,0:T(8,128)(2,1)}), bf16[2048,512]{1,0:T(8,128)(2,1)}) %all-gather.22.cloned.1.call-update) | async-done | bytes 2097168 | tf_op jit(solution)/shard_map/all_gather | solution.py:96
  203.4 3.2 constant_dynamic-update-slice_fusion.2
  206.6 39.0 %all-gather.24.cloned.1.call-done = bf16[2048,512]{1,0:T(8,128)(2,1)} async-done(((bf16[128,512]{1,0:T(8,128)(2,1)}), bf16[2048,512]{1,0:T(8,128)(2,1)}) %all-gather.24.cloned.1.call-update) | async-done | bytes 2097168 | tf_op jit(solution)/shard_map/all_gather | solution.py:97
  245.6 3.2 constant_dynamic-update-slice_fusion.1
  248.8 39.1 %all-gather.26.cloned.1.call-done = bf16[2048,512]{1,0:T(8,128)(2,1)} async-done(((bf16[128,512]{1,0:T(8,128)(2,1)}), bf16[2048,512]{1,0:T(8,128)(2,1)}) %all-gather.26.cloned.1.call-update) | async-done | bytes 2097168 | tf_op jit(solution)/shard_map/all_gather | solution.py:98
  288.0 3.1 constant_dynamic-update-slice_fusion
  291.1 8.0 %fusion.29 = bf16[256,3072]{1,0:T(8,128)(2,1)S(1)} fusion(bf16[2048,3072]{1,0:T(8,128)(2,1)} %constant_dynamic-update-slice_fusion, f32[256]{0:T(256)S(1)} %add_rsqrt_fusion.1, bf16[256,2048]{1,0:T(8,128)(2,1)S(1)} %copy-done.3, f32[2048]{0:T(1024)S(1)} %copy-done.10), kind=kOutput, calls=%fused_computation.44 | convolution fusion | flops 3224371200 | bytes 15213568 | tf_op jit(solution)/shard_map/dot_general | solution.py:106
  299.1 1.0 slice_convert_fusion.1
  301.9 48.2 %while.30 = (s32[]{:T(128)}, f32[4,128,128]{2,1,0:T(8,128)S(1)}, f32[4,128]{1,0:T(4,128)S(1)}, f32[4,4,64,128]{3,2,0,1:T(8,128)}, f32[4,4,64,128]{3,2,0,1:T(8,12...) while((s32[]{:T(128)}, f32[4,128,128]{2,1,0:T(8,128)S(1)}, ...), condition=%wide.region_3.4_spmd.clone, body=%wide.region_1.3_spmd.clone.sunk | while | flops 140923904 | bytes 20806288 | solution.py:68
  302.3 1.7 exponential_select_fusion.2
  304.0 7.3 %fusion.136 = f32[4,64,64]{1,2,0:T(8,128)S(1)} fusion(f32[4,64,64,128]{3,2,1,0:T(8,128)S(1)} %exponential_select_fusion.2, f32[4,128,64]{1,2,0:T(8,128)S(1)} %dynamic-slice_bitcast_fusion.9, f32[4,128,64]{1,2,0:T(8,128)S(1)} %get-tuple-element.298), kind=kLoop, calls=%fused_computation.4.clone.1 | loop fusion | flops 6275072 | bytes 8716288 | tf_op jit(solution)/shard_map/while/body/eval_jaxpr/htk,hsk,htsk->hts/dot_general | solution.py:52
  311.3 0.4 fusion.137
  311.7 1.0 fusion.138
  312.8 0.7 convolution_add_fusion.3
  313.4 0.7 bitcast_dynamic-update-slice_fusion.2
  314.3 1.7 exponential_select_fusion.2
  316.0 7.3 %fusion.136 = f32[4,64,64]{1,2,0:T(8,128)S(1)} fusion(f32[4,64,64,128]{3,2,1,0:T(8,128)S(1)} %exponential_select_fusion.2, f32[4,128,64]{1,2,0:T(8,128)S(1)} %dynamic-slice_bitcast_fusion.9, f32[4,128,64]{1,2,0:T(8,128)S(1)} %get-tuple-element.298), kind=kLoop, calls=%fused_computation.4.clone.1 | loop fusion | flops 6275072 | bytes 8716288 | tf_op jit(solution)/shard_map/while/body/eval_jaxpr/htk,hsk,htsk->hts/dot_general | solution.py:52
  323.3 0.4 fusion.137
  323.7 1.0 fusion.138
  324.8 0.7 convolution_add_fusion.3
  325.5 0.7 bitcast_dynamic-update-slice_fusion.2
  326.3 1.7 exponential_select_fusion.2
  328.0 7.3 %fusion.136 = f32[4,64,64]{1,2,0:T(8,128)S(1)} fusion(f32[4,64,64,128]{3,2,1,0:T(8,128)S(1)} %exponential_select_fusion.2, f32[4,128,64]{1,2,0:T(8,128)S(1)} %dynamic-slice_bitcast_fusion.9, f32[4,128,64]{1,2,0:T(8,128)S(1)} %get-tuple-element.298), kind=kLoop, calls=%fused_computation.4.clone.1 | loop fusion | flops 6275072 | bytes 8716288 | tf_op jit(solution)/shard_map/while/body/eval_jaxpr/htk,hsk,htsk->hts/dot_general | solution.py:52
  335.7 1.0 fusion.138
  336.8 0.7 convolution_add_fusion.3
  337.5 0.7 bitcast_dynamic-update-slice_fusion.2
  338.3 1.7 exponential_select_fusion.2
  340.0 7.3 %fusion.136 = f32[4,64,64]{1,2,0:T(8,128)S(1)} fusion(f32[4,64,64,128]{3,2,1,0:T(8,128)S(1)} %exponential_select_fusion.2, f32[4,128,64]{1,2,0:T(8,128)S(1)} %dynamic-slice_bitcast_fusion.9, f32[4,128,64]{1,2,0:T(8,128)S(1)} %get-tuple-element.298), kind=kLoop, calls=%fused_computation.4.clone.1 | loop fusion | flops 6275072 | bytes 8716288 | tf_op jit(solution)/shard_map/while/body/eval_jaxpr/htk,hsk,htsk->hts/dot_general | solution.py:52
  347.7 1.0 fusion.138
  348.8 0.7 convolution_add_fusion.3
  349.5 0.7 bitcast_dynamic-update-slice_fusion.2
  350.1 0.7 copy-done.1
  350.9 0.7 all-gather.28.cloned.1.call-update
  351.7 0.5 all-gather.30.cloned.1.call-update
  352.5 0.7 slice.99
  353.2 2.1 collective-permute-start
  355.4 19.7 %all-gather.2 = f32[16,4,128]{2,1,0:T(4,128)S(1)} all-gather(f32[1,4,128]{2,1,0:T(4,128)S(1)} %exponential_bitcast_fusion), channel_id=2, replica_groups=mesh['sp'=16,'tp'=2] {'sp'}, dimensions={0}, use_global_device_ids=true | all-gather | bytes 34816 | tf_op jit(solution)/shard_map/all_gather | solution.py:14
  375.1 1.7 fusion.103
  377.0 23.2 %all-gather.32.cloned.1.call-done = f32[64,128,128]{2,1,0:T(8,128)} async-done(((f32[4,128,128]{2,1,0:T(8,128)}), f32[64,128,128]{2,1,0:T(8,128)}) %all-gather.32.cloned.1.call-update) | async-done | bytes 4194320 | tf_op jit(solution)/shard_map/all_gather | solution.py:14
  400.3 0.7 multiply_reduce_fusion
  401.8 1.4 fusion.101
  403.2 38.8 %all-gather.28.cloned.1.call-done = bf16[512,2048]{1,0:T(8,128)(2,1)} async-done(((bf16[512,128]{1,0:T(8,128)(2,1)}), bf16[512,2048]{1,0:T(8,128)(2,1)}) %all-gather.28.cloned.1.call-update) | async-done | bytes 2097168 | tf_op jit(solution)/shard_map/all_gather | solution.py:173
  442.0 42.2 %all-gather.30.cloned.1.call-done = bf16[512,2048]{1,0:T(8,128)(2,1)} async-done(((bf16[512,128]{1,0:T(8,128)(2,1)}), bf16[512,2048]{1,0:T(8,128)(2,1)}) %all-gather.30.cloned.1.call-update) | async-done | bytes 2097168 | tf_op jit(solution)/shard_map/all_gather | solution.py:174
  484.1 4.5 fusion.30
  488.6 19.6 %reduce-scatter.2.cloned.1.call-done = bf16[128,2048]{1,0:T(8,128)(2,1)} async-done(((bf16[256,2048]{1,0:T(8,128)(2,1)}), bf16[128,2048]{1,0:T(8,128)(2,1)}) %reduce-scatter.2.cloned.1.call-update) | async-done | bytes 524304 | tf_op jit(solution)/shard_map/reduce_scatter | solution.py:178
  508.3 1.2 fusion.37
  509.5 2.0 fusion.39
  (94 shorter events, 5.0 us)
Async XLA Ops:
  6.5 368.5 %copy-start = (bf16[4,128,128]{2,1,0:T(8,128)(2,1)S(1)}, bf16[4,128,128]{2,1,0:T(8,128)(2,1)}, u32[]{:S(2)}) copy-start(bf16[4,128,128]{2,1,0:T(8,128)(2,1)} %param.31) | copy-start | bytes 393220
  6.5 26.4 %all-gather.14.cloned.1.call-start = ((), (), s32[]{:S(2)}) async-start(), calls=%async_computation.1 | async-start | bytes 1572864 | tf_op jit(solution)/shard_map/all_gather | solution.py:104
  7.3 69.3 %all-gather.16.cloned.1.call-start = ((), (), s32[]{:S(2)}) async-start(), calls=%async_computation.2 | async-start | bytes 2228224 | tf_op jit(solution)/shard_map/all_gather | solution.py:93
  8.0 110.9 %all-gather.18.cloned.1.call-start = ((), (), s32[]{:S(2)}) async-start(), calls=%async_computation.3 | async-start | bytes 2228224 | tf_op jit(solution)/shard_map/all_gather | solution.py:94
  8.7 152.4 %all-gather.20.cloned.1.call-start = ((), (), s32[]{:S(2)}) async-start(), calls=%async_computation.4 | async-start | bytes 2228224 | tf_op jit(solution)/shard_map/all_gather | solution.py:95
  9.3 194.1 %all-gather.22.cloned.1.call-start = ((), (), s32[]{:S(2)}) async-start(), calls=%async_computation.5 | async-start | bytes 2228224 | tf_op jit(solution)/shard_map/all_gather | solution.py:96
  9.9 235.7 %all-gather.24.cloned.1.call-start = ((), (), s32[]{:S(2)}) async-start(), calls=%async_computation.6 | async-start | bytes 2228224 | tf_op jit(solution)/shard_map/all_gather | solution.py:97
  10.5 277.5 %all-gather.26.cloned.1.call-start = ((), (), s32[]{:S(2)}) async-start(), calls=%async_computation.7 | async-start | bytes 2228224 | tf_op jit(solution)/shard_map/all_gather | solution.py:98
  11.2 389.0 %all-gather.32.cloned.1.call-start = ((), (), s32[]{:S(2)}) async-start(), calls=%async_computation.11 | async-start | bytes 4456448 | tf_op jit(solution)/shard_map/all_gather | solution.py:14
  206.6 84.5 %copy-start.3 = (bf16[256,2048]{1,0:T(8,128)(2,1)S(1)}, bf16[256,2048]{1,0:T(8,128)(2,1)}, u32[]{:S(2)}) copy-start(bf16[256,2048]{1,0:T(8,128)(2,1)} %all-gather.14.cloned.1.call-done) | copy-start | bytes 3145732
  206.6 84.5 %copy-start.10 = (f32[2048]{0:T(1024)S(1)}, f32[2048]{0:T(1024)}, u32[]{:S(2)}) copy-start(f32[2048]{0:T(1024)} %param.21) | copy-start | bytes 24580
  299.1 1.7 copy-start.2
  301.9 73.2 %copy-start.4 = (f32[256,512]{1,0:T(8,128)S(1)}, f32[256,512]{1,0:T(8,128)}, u32[]{:S(2)}) copy-start(f32[256,512]{1,0:T(8,128)} %get-tuple-element.180) | copy-start | bytes 1572868
  350.1 0.7 copy-start.1
  350.9 91.1 %all-gather.28.cloned.1.call-start = ((), (), s32[]{:S(2)}) async-start(), calls=%async_computation.8 | async-start | bytes 2228224 | tf_op jit(solution)/shard_map/all_gather | solution.py:173
  351.6 132.5 %all-gather.30.cloned.1.call-start = ((), (), s32[]{:S(2)}) async-start(), calls=%async_computation.9 | async-start | bytes 2228224 | tf_op jit(solution)/shard_map/all_gather | solution.py:174
  352.2 156.1 %reduce-scatter.2.cloned.1.call-start = ((), (), s32[]{:S(2)}) async-start(), calls=%async_computation.10 | async-start | bytes 1572864 | tf_op jit(solution)/shard_map/reduce_scatter | solution.py:178
  353.2 21.8 %collective-permute-start = (bf16[16,512]{1,0:T(8,128)(2,1)S(1)}, bf16[16,512]{1,0:T(8,128)(2,1)S(1)}, u32[]{:S(2)}, u32[]{:S(2)}) collective-permute-start(bf16[16,512]{1,0:T(8,128)(2,1)S(1)} %slice.99), channel_id=1, source_target_pairs={{0,2},{2,4},{4,6},{6,8},{8,10},{10,12},{12,14},{14,16},{16,18},{18... | collective-permute-start | bytes 49160 | tf_op jit(solution)/shard_map/ppermute | solution.py:28
  376.8 23.4 %copy-start.5 = (f32[4,4,64,128]{3,2,0,1:T(8,128)S(1)}, f32[4,4,64,128]{3,2,0,1:T(8,128)}, u32[]{:S(2)}) copy-start(f32[4,4,64,128]{3,2,0,1:T(8,128)} %get-tuple-element.104) | copy-start | bytes 1572868
  376.8 23.4 %copy-start.6 = (f32[4,4,64,128]{3,2,0,1:T(8,128)S(1)}, f32[4,4,64,128]{3,2,0,1:T(8,128)}, u32[]{:S(2)}) copy-start(f32[4,4,64,128]{3,2,0,1:T(8,128)} %get-tuple-element.108) | copy-start | bytes 1572868
  377.0 24.8 %copy-start.8 = (f32[512]{0:T(512)S(1)}, f32[512]{0:T(512)}, u32[]{:S(2)}) copy-start(f32[512]{0:T(512)} %param.30) | copy-start | bytes 6148
  377.0 24.8 %copy-start.9 = (f32[512]{0:T(512)S(1)}, f32[512]{0:T(512)}, u32[]{:S(2)}) copy-start(f32[512]{0:T(512)} %param.32) | copy-start | bytes 6148
  484.1 25.4 %copy-start.7 = (f32[2048]{0:T(1024)S(1)}, f32[2048]{0:T(1024)}, u32[]{:S(2)}) copy-start(f32[2048]{0:T(1024)} %param.35) | copy-start | bytes 24580
Sparse Core Ops, SparseCore 0:
  8.9 23.9 all-gather.13
  35.1 41.4 all-gather.15
  78.7 40.1 all-gather.17
  121.0 40.1 all-gather.19
  163.2 40.1 all-gather.21
  205.4 40.1 all-gather.23
  247.8 40.1 all-gather.25
  351.0 49.1 all-gather.31
  402.4 39.5 all-gather.27
  444.0 40.1 all-gather.29
  488.8 19.4 reduce-scatter.1
where the time goes:
time: 519 us; the launch traced here: 518 us
  waiting for transfers between devices  387 us (75%)
  other arithmetic  47.9 us (9%)
  local copies, waits for them, and re-layouts  23.9 us (5%)
  matrix products  23.2 us (4%)
  blocking collectives  19.7 us (4%)
  between operations  13.6 us (3%)
    all_gather x1, waiting for transfers between devices, per_device(): lax.all_gather(out_pool, 'sp', axis=1, tiled=True)  42.2 us
    all_gather x1, waiting for transfers between devices, per_device(): lax.all_gather(w_query, 'sp', axis=0, tiled=True)  42.1 us
    all_gather x1, waiting for transfers between devices, per_device(): lax.all_gather(w_forget, 'sp', axis=0, tiled=True)  39.2 us
    all_gather x1, waiting for transfers between devices, per_device(): lax.all_gather(w_pgate, 'sp', axis=0, tiled=True)  39.1 us
    all_gather x1, waiting for transfers between devices, per_device(): lax.all_gather(w_rgate, 'sp', axis=0, tiled=True)  39.1 us
    all_gather x1, waiting for transfers between devices, per_device(): lax.all_gather(w_pool_in, 'sp', axis=0, tiled=True)  39 us
    all_gather x1, waiting for transfers between devices, per_device(): lax.all_gather(w_input, 'sp', axis=0, tiled=True)  39 us
    all_gather x1, waiting for transfers between devices, per_device(): lax.all_gather(out_rec, 'sp', axis=1, tiled=True)  38.8 us
  transfers between devices with their start and end apart: 12, of which 11 were waited for; matrix products, arithmetic and copies ran while one was open for 5% of the time, Pallas kernels for 0%

commit v1 on v0

--- a/solution.py
+++ b/solution.py
@@ -91,7 +91,9 @@
 ):
     gathered = (
         lax.all_gather(w_query, "sp", axis=0, tiled=True),
-        lax.all_gather(w_forget, "sp", axis=0, tiled=True),
+        jnp.concatenate(
+            lax.all_to_all(jnp.stack([w_forget] * lax.axis_size("sp")), "sp", 0, 0), axis=0
+        ),
         lax.all_gather(w_input, "sp", axis=0, tiled=True),
         lax.all_gather(w_rgate, "sp", axis=0, tiled=True),
         lax.all_gather(w_pool_in, "sp", axis=0, tiled=True),

time: 519 us -> 487 us (0.938)
  waiting for transfers between devices: 387 us -> 348 us
  starting transfers between devices: 2.51 us -> 9.89 us
    all_gather x1 -> x0, waiting for transfers between devices: 39.2 us -> none  [per_device(): lax.all_gather(w_forget, 'sp', axis=0, tiled=True)]
    all_gather x1, waiting for transfers between devices: 42.1 us -> 51.7 us  [per_device(): lax.all_gather(w_query, 'sp', axis=0, tiled=True)]
    all_gather x1, waiting for transfers between devices: 20.1 us -> 12.2 us  [per_device(): lax.all_gather(tokens_in, 'tp', axis=1, tiled=True).astype(jnp.float32)]
    all_to_all x0 -> x1, starting transfers between devices: none -> 7.41 us  [per_device(): lax.all_to_all(jnp.stack([w_forget] * lax.axis_size('sp')), 'sp', 0, 0)]
    unnamed x29 -> x33, local copies, waits for them, and re-layouts: 17.6 us -> 15.2 us
  transfers between devices with their start and end apart: 12 -> 12, of which waited for: 11 -> 10; matrix products, arithmetic and copies ran while one was open for 5% -> 5% of each run, Pallas kernels for 0% -> 0%
where the time goes in v1:
time: 487 us; the launch traced here: 486 us
  waiting for transfers between devices  348 us (71%)
  other arithmetic  47.3 us (10%)
  local copies, waits for them, and re-layouts  24.1 us (5%)
  matrix products  23.2 us (5%)
  blocking collectives  19.8 us (4%)
  between operations  13.9 us (3%)
  starting transfers between devices  9.89 us (2%)
    all_gather x1, waiting for transfers between devices, per_device(): lax.all_gather(w_query, 'sp', axis=0, tiled=True)  51.7 us
    all_gather x1, waiting for transfers between devices, per_device(): lax.all_gather(out_pool, 'sp', axis=1, tiled=True)  42.3 us
    all_gather x1, waiting for transfers between devices, per_device(): lax.all_gather(w_pool_in, 'sp', axis=0, tiled=True)  39.1 us
    all_gather x1, waiting for transfers between devices, per_device(): lax.all_gather(w_pgate, 'sp', axis=0, tiled=True)  39.1 us
    all_gather x1, waiting for transfers between devices, per_device(): lax.all_gather(w_rgate, 'sp', axis=0, tiled=True)  39 us
    all_gather x1, waiting for transfers between devices, per_device(): lax.all_gather(out_rec, 'sp', axis=1, tiled=True)  38.7 us
    all_gather x1, waiting for transfers between devices, per_device(): lax.all_gather(w_input, 'sp', axis=0, tiled=True)  38 us
    dot_general x4, other arithmetic, advance(): jnp.einsum('htk,hsk,htsk->hts', probe_segment, key_piece, weight, precisi...  29.3 us
  transfers between devices with their start and end apart: 12, of which 10 were waited for; matrix products, arithmetic and copies ran while one was open for 5% of the time, Pallas kernels for 0%

profile of v1, /device:TPU:0, one launch (start us, length us, event | category | flops | bytes accessed | tf_op | source)
XLA Modules:
  0.0 486.3 jit_solution(6207463690552763551)
XLA Ops:
  6.5 0.7 all-gather.13.cloned.1.call-update
  7.3 0.7 all-gather.15.cloned.1.call-update
  8.1 0.7 all-gather.17.cloned.1.call-update
  8.8 0.5 all-gather.19.cloned.1.call-update
  9.4 0.5 all-gather.21.cloned.1.call-update
  9.9 2.5 stack.2
  12.4 7.4 %all-to-all-start = ((bf16[16,128,512]{2,1,0:T(8,128)(2,1)}), bf16[16,128,512]{2,1,0:T(8,128)(2,1)S(1)}, u32[]{:S(2)}, u32[]{:S(2)}) async-start(bf16[16,128,512]{2,1,0:T(8,128)(2,1)} %stack.2), calls=%async_computation | async-start | bytes 4194304 | tf_op jit(solution)/shard_map/all_to_all | solution.py:95
  19.9 0.5 all-gather.23.cloned.1.call-update
  20.7 12.2 %all-gather.13.cloned.1.call-done = bf16[256,2048]{1,0:T(8,128)(2,1)} async-done(((bf16[256,1024]{1,0:T(8,128)(2,1)}), bf16[256,2048]{1,0:T(8,128)(2,1)}) %all-gather.13.cloned.1.call-update) | async-done | bytes 1048592 | tf_op jit(solution)/shard_map/all_gather | solution.py:106
  32.9 1.5 fusion.34
  34.4 51.7 %all-gather.15.cloned.1.call-done = bf16[2048,512]{1,0:T(8,128)(2,1)} async-done(((bf16[128,512]{1,0:T(8,128)(2,1)}), bf16[2048,512]{1,0:T(8,128)(2,1)}) %all-gather.15.cloned.1.call-update) | async-done | bytes 2097168 | tf_op jit(solution)/shard_map/all_gather | solution.py:93
  86.2 3.1 constant_dynamic-update-slice_fusion.5
  89.3 1.6 constant_dynamic-update-slice_fusion.4
  90.9 38.0 %all-gather.17.cloned.1.call-done = bf16[2048,512]{1,0:T(8,128)(2,1)} async-done(((bf16[128,512]{1,0:T(8,128)(2,1)}), bf16[2048,512]{1,0:T(8,128)(2,1)}) %all-gather.17.cloned.1.call-update) | async-done | bytes 2097168 | tf_op jit(solution)/shard_map/all_gather | solution.py:97
  128.9 3.2 constant_dynamic-update-slice_fusion.3
  132.1 39.0 %all-gather.19.cloned.1.call-done = bf16[2048,512]{1,0:T(8,128)(2,1)} async-done(((bf16[128,512]{1,0:T(8,128)(2,1)}), bf16[2048,512]{1,0:T(8,128)(2,1)}) %all-gather.19.cloned.1.call-update) | async-done | bytes 2097168 | tf_op jit(solution)/shard_map/all_gather | solution.py:98
  171.1 3.1 constant_dynamic-update-slice_fusion.2
  174.3 39.1 %all-gather.21.cloned.1.call-done = bf16[2048,512]{1,0:T(8,128)(2,1)} async-done(((bf16[128,512]{1,0:T(8,128)(2,1)}), bf16[2048,512]{1,0:T(8,128)(2,1)}) %all-gather.21.cloned.1.call-update) | async-done | bytes 2097168 | tf_op jit(solution)/shard_map/all_gather | solution.py:99
  213.4 3.2 constant_dynamic-update-slice_fusion.1
  216.5 39.1 %all-gather.23.cloned.1.call-done = bf16[2048,512]{1,0:T(8,128)(2,1)} async-done(((bf16[128,512]{1,0:T(8,128)(2,1)}), bf16[2048,512]{1,0:T(8,128)(2,1)}) %all-gather.23.cloned.1.call-update) | async-done | bytes 2097168 | tf_op jit(solution)/shard_map/all_gather | solution.py:100
  255.6 3.2 constant_dynamic-update-slice_fusion
  258.8 8.0 %fusion.29 = bf16[256,3072]{1,0:T(8,128)(2,1)S(1)} fusion(bf16[2048,3072]{1,0:T(8,128)(2,1)} %constant_dynamic-update-slice_fusion, f32[256]{0:T(256)S(1)} %add_rsqrt_fusion.1, bf16[256,2048]{1,0:T(8,128)(2,1)S(1)} %copy-done.3, f32[2048]{0:T(1024)S(1)} %copy-done.12), kind=kOutput, calls=%fused_computation.44 | convolution fusion | flops 3224371200 | bytes 15213568 | tf_op jit(solution)/shard_map/dot_general | solution.py:108
  266.8 1.0 slice_convert_fusion.1
  269.6 48.3 %while.30 = (s32[]{:T(128)}, f32[4,128,128]{2,1,0:T(8,128)S(1)}, f32[4,128]{1,0:T(4,128)S(1)}, f32[4,4,64,128]{3,2,0,1:T(8,128)}, f32[4,4,64,128]{3,2,0,1:T(8,12...) while((s32[]{:T(128)}, f32[4,128,128]{2,1,0:T(8,128)S(1)}, ...), condition=%wide.region_3.4_spmd.clone, body=%wide.region_1.3_spmd.clone.sunk | while | flops 140923904 | bytes 20806288 | solution.py:68
  270.0 1.7 exponential_select_fusion.2
  271.7 7.3 %fusion.136 = f32[4,64,64]{1,2,0:T(8,128)S(1)} fusion(f32[4,64,64,128]{3,2,1,0:T(8,128)S(1)} %exponential_select_fusion.2, f32[4,128,64]{1,2,0:T(8,128)S(1)} %dynamic-slice_bitcast_fusion.9, f32[4,128,64]{1,2,0:T(8,128)S(1)} %get-tuple-element.298), kind=kLoop, calls=%fused_computation.4.clone.1 | loop fusion | flops 6275072 | bytes 8716288 | tf_op jit(solution)/shard_map/while/body/eval_jaxpr/htk,hsk,htsk->hts/dot_general | solution.py:52
  279.0 0.4 fusion.137
  279.4 1.0 fusion.138
  280.5 0.7 convolution_add_fusion.3
  281.2 0.7 bitcast_dynamic-update-slice_fusion.2
  282.0 1.7 exponential_select_fusion.2
  283.7 7.3 %fusion.136 = f32[4,64,64]{1,2,0:T(8,128)S(1)} fusion(f32[4,64,64,128]{3,2,1,0:T(8,128)S(1)} %exponential_select_fusion.2, f32[4,128,64]{1,2,0:T(8,128)S(1)} %dynamic-slice_bitcast_fusion.9, f32[4,128,64]{1,2,0:T(8,128)S(1)} %get-tuple-element.298), kind=kLoop, calls=%fused_computation.4.clone.1 | loop fusion | flops 6275072 | bytes 8716288 | tf_op jit(solution)/shard_map/while/body/eval_jaxpr/htk,hsk,htsk->hts/dot_general | solution.py:52
  291.1 0.4 fusion.137
  291.5 1.0 fusion.138
  292.5 0.7 convolution_add_fusion.3
  293.2 0.7 bitcast_dynamic-update-slice_fusion.2
  294.0 1.7 exponential_select_fusion.2
  295.8 7.3 %fusion.136 = f32[4,64,64]{1,2,0:T(8,128)S(1)} fusion(f32[4,64,64,128]{3,2,1,0:T(8,128)S(1)} %exponential_select_fusion.2, f32[4,128,64]{1,2,0:T(8,128)S(1)} %dynamic-slice_bitcast_fusion.9, f32[4,128,64]{1,2,0:T(8,128)S(1)} %get-tuple-element.298), kind=kLoop, calls=%fused_computation.4.clone.1 | loop fusion | flops 6275072 | bytes 8716288 | tf_op jit(solution)/shard_map/while/body/eval_jaxpr/htk,hsk,htsk->hts/dot_general | solution.py:52
  303.1 0.4 fusion.137
  303.5 1.0 fusion.138
  304.5 0.7 convolution_add_fusion.3
  305.2 0.7 bitcast_dynamic-update-slice_fusion.2
  306.1 1.7 exponential_select_fusion.2
  307.8 7.3 %fusion.136 = f32[4,64,64]{1,2,0:T(8,128)S(1)} fusion(f32[4,64,64,128]{3,2,1,0:T(8,128)S(1)} %exponential_select_fusion.2, f32[4,128,64]{1,2,0:T(8,128)S(1)} %dynamic-slice_bitcast_fusion.9, f32[4,128,64]{1,2,0:T(8,128)S(1)} %get-tuple-element.298), kind=kLoop, calls=%fused_computation.4.clone.1 | loop fusion | flops 6275072 | bytes 8716288 | tf_op jit(solution)/shard_map/while/body/eval_jaxpr/htk,hsk,htsk->hts/dot_general | solution.py:52
  315.1 0.4 fusion.137
  315.5 1.0 fusion.138
  316.6 0.7 convolution_add_fusion.3
  317.2 0.7 bitcast_dynamic-update-slice_fusion.2
  317.9 0.7 copy-done.1
  318.7 0.7 all-gather.25.cloned.1.call-update
  319.5 0.7 all-gather.27.cloned.1.call-update
  320.4 0.7 slice.99
  321.2 2.1 collective-permute-start
  323.3 19.8 %all-gather.2 = f32[16,4,128]{2,1,0:T(4,128)S(1)} all-gather(f32[1,4,128]{2,1,0:T(4,128)S(1)} %exponential_bitcast_fusion), channel_id=2, replica_groups=mesh['sp'=16,'tp'=2] {'sp'}, dimensions={0}, use_global_device_ids=true | all-gather | bytes 34816 | tf_op jit(solution)/shard_map/all_gather | solution.py:14
  343.1 1.7 fusion.103
  345.1 22.9 %all-gather.29.cloned.1.call-done = f32[64,128,128]{2,1,0:T(8,128)} async-done(((f32[4,128,128]{2,1,0:T(8,128)}), f32[64,128,128]{2,1,0:T(8,128)}) %all-gather.29.cloned.1.call-update) | async-done | bytes 4194320 | tf_op jit(solution)/shard_map/all_gather | solution.py:14
  368.0 0.7 multiply_reduce_fusion
  369.6 1.4 fusion.101
  371.0 38.7 %all-gather.25.cloned.1.call-done = bf16[512,2048]{1,0:T(8,128)(2,1)} async-done(((bf16[512,128]{1,0:T(8,128)(2,1)}), bf16[512,2048]{1,0:T(8,128)(2,1)}) %all-gather.25.cloned.1.call-update) | async-done | bytes 2097168 | tf_op jit(solution)/shard_map/all_gather | solution.py:175
  409.7 42.3 %all-gather.27.cloned.1.call-done = bf16[512,2048]{1,0:T(8,128)(2,1)} async-done(((bf16[512,128]{1,0:T(8,128)(2,1)}), bf16[512,2048]{1,0:T(8,128)(2,1)}) %all-gather.27.cloned.1.call-update) | async-done | bytes 2097168 | tf_op jit(solution)/shard_map/all_gather | solution.py:176
  452.1 4.5 fusion.30
  456.6 19.6 %reduce-scatter.2.cloned.1.call-done = bf16[128,2048]{1,0:T(8,128)(2,1)} async-done(((bf16[256,2048]{1,0:T(8,128)(2,1)}), bf16[128,2048]{1,0:T(8,128)(2,1)}) %reduce-scatter.2.cloned.1.call-update) | async-done | bytes 524304 | tf_op jit(solution)/shard_map/reduce_scatter | solution.py:180
  476.2 1.2 fusion.37
  477.5 2.0 fusion.39
  (98 shorter events, 4.4 us)
Async XLA Ops:
  6.5 336.6 %copy-start = (bf16[4,128,128]{2,1,0:T(8,128)(2,1)S(1)}, bf16[4,128,128]{2,1,0:T(8,128)(2,1)}, u32[]{:S(2)}) copy-start(bf16[4,128,128]{2,1,0:T(8,128)(2,1)} %param.31) | copy-start | bytes 393220
  6.5 14.0 %copy-start.8 = (f32[256,4]{0,1:T(4,128)S(1)}, f32[256,4]{0,1:T(4,128)}, u32[]{:S(2)}) copy-start(f32[256,4]{0,1:T(4,128)} %param.29) | copy-start | bytes 12292
  6.5 14.1 %copy-start.11 = (f32[512]{0:T(512)S(1)}, f32[512]{0:T(512)}, u32[]{:S(2)}) copy-start(f32[512]{0:T(512)} %param.28) | copy-start | bytes 6148
  6.5 26.4 %all-gather.13.cloned.1.call-start = ((), (), s32[]{:S(2)}) async-start(), calls=%async_computation.2 | async-start | bytes 1572864 | tf_op jit(solution)/shard_map/all_gather | solution.py:106
  7.3 78.9 %all-gather.15.cloned.1.call-start = ((), (), s32[]{:S(2)}) async-start(), calls=%async_computation.3 | async-start | bytes 2228224 | tf_op jit(solution)/shard_map/all_gather | solution.py:93
  8.0 120.9 %all-gather.17.cloned.1.call-start = ((), (), s32[]{:S(2)}) async-start(), calls=%async_computation.4 | async-start | bytes 2228224 | tf_op jit(solution)/shard_map/all_gather | solution.py:97
  8.7 162.4 %all-gather.19.cloned.1.call-start = ((), (), s32[]{:S(2)}) async-start(), calls=%async_computation.5 | async-start | bytes 2228224 | tf_op jit(solution)/shard_map/all_gather | solution.py:98
  9.3 204.0 %all-gather.21.cloned.1.call-start = ((), (), s32[]{:S(2)}) async-start(), calls=%async_computation.6 | async-start | bytes 2228224 | tf_op jit(solution)/shard_map/all_gather | solution.py:99
  12.4 76.9 %all-to-all-start = ((bf16[16,128,512]{2,1,0:T(8,128)(2,1)}), bf16[16,128,512]{2,1,0:T(8,128)(2,1)S(1)}, u32[]{:S(2)}, u32[]{:S(2)}) async-start(bf16[16,128,512]{2,1,0:T(8,128)(2,1)} %stack.2), calls=%async_computation | async-start | bytes 4194304 | tf_op jit(solution)/shard_map/all_to_all | solution.py:95
  19.8 235.7 %all-gather.23.cloned.1.call-start = ((), (), s32[]{:S(2)}) async-start(), calls=%async_computation.7 | async-start | bytes 2228224 | tf_op jit(solution)/shard_map/all_gather | solution.py:100
  20.4 347.6 %all-gather.29.cloned.1.call-start = ((), (), s32[]{:S(2)}) async-start(), calls=%async_computation.11 | async-start | bytes 4456448 | tf_op jit(solution)/shard_map/all_gather | solution.py:14
  174.3 84.5 %copy-start.3 = (bf16[256,2048]{1,0:T(8,128)(2,1)S(1)}, bf16[256,2048]{1,0:T(8,128)(2,1)}, u32[]{:S(2)}) copy-start(bf16[256,2048]{1,0:T(8,128)(2,1)} %all-gather.13.cloned.1.call-done) | copy-start | bytes 3145732
  174.3 84.5 %copy-start.12 = (f32[2048]{0:T(1024)S(1)}, f32[2048]{0:T(1024)}, u32[]{:S(2)}) copy-start(f32[2048]{0:T(1024)} %param.21) | copy-start | bytes 24580
  266.8 1.7 copy-start.2
  269.6 73.5 %copy-start.4 = (f32[256,512]{1,0:T(8,128)S(1)}, f32[256,512]{1,0:T(8,128)}, u32[]{:S(2)}) copy-start(f32[256,512]{1,0:T(8,128)} %get-tuple-element.180) | copy-start | bytes 1572868
  317.9 0.7 copy-start.1
  318.7 91.1 %all-gather.25.cloned.1.call-start = ((), (), s32[]{:S(2)}) async-start(), calls=%async_computation.8 | async-start | bytes 2228224 | tf_op jit(solution)/shard_map/all_gather | solution.py:175
  319.4 132.6 %all-gather.27.cloned.1.call-start = ((), (), s32[]{:S(2)}) async-start(), calls=%async_computation.9 | async-start | bytes 2228224 | tf_op jit(solution)/shard_map/all_gather | solution.py:176
  320.1 156.1 %reduce-scatter.2.cloned.1.call-start = ((), (), s32[]{:S(2)}) async-start(), calls=%async_computation.10 | async-start | bytes 1572864 | tf_op jit(solution)/shard_map/reduce_scatter | solution.py:180
  321.2 21.9 %collective-permute-start = (bf16[16,512]{1,0:T(8,128)(2,1)S(1)}, bf16[16,512]{1,0:T(8,128)(2,1)S(1)}, u32[]{:S(2)}, u32[]{:S(2)}) collective-permute-start(bf16[16,512]{1,0:T(8,128)(2,1)S(1)} %slice.99), channel_id=1, source_target_pairs={{0,2},{2,4},{4,6},{6,8},{8,10},{10,12},{12,14},{14,16},{16,18},{18... | collective-permute-start | bytes 49160 | tf_op jit(solution)/shard_map/ppermute | solution.py:28
  344.8 23.2 %copy-start.5 = (f32[4,4,64,128]{3,2,0,1:T(8,128)S(1)}, f32[4,4,64,128]{3,2,0,1:T(8,128)}, u32[]{:S(2)}) copy-start(f32[4,4,64,128]{3,2,0,1:T(8,128)} %get-tuple-element.104) | copy-start | bytes 1572868
  344.8 23.2 %copy-start.6 = (f32[4,4,64,128]{3,2,0,1:T(8,128)S(1)}, f32[4,4,64,128]{3,2,0,1:T(8,128)}, u32[]{:S(2)}) copy-start(f32[4,4,64,128]{3,2,0,1:T(8,128)} %get-tuple-element.108) | copy-start | bytes 1572868
  345.0 24.6 %copy-start.9 = (f32[512]{0:T(512)S(1)}, f32[512]{0:T(512)}, u32[]{:S(2)}) copy-start(f32[512]{0:T(512)} %param.30) | copy-start | bytes 6148
  345.0 24.6 %copy-start.10 = (f32[512]{0:T(512)S(1)}, f32[512]{0:T(512)}, u32[]{:S(2)}) copy-start(f32[512]{0:T(512)} %param.32) | copy-start | bytes 6148
  452.0 25.4 %copy-start.7 = (f32[2048]{0:T(1024)S(1)}, f32[2048]{0:T(1024)}, u32[]{:S(2)}) copy-start(f32[2048]{0:T(1024)} %param.35) | copy-start | bytes 24580
Sparse Core Ops, SparseCore 0:
  8.9 23.9 all-gather.12
  35.1 51.0 all-gather.14
  88.3 40.5 all-gather.16
  130.9 40.1 all-gather.18
  173.1 40.1 all-gather.20
  215.4 40.1 all-gather.22
  318.8 49.1 all-gather.28
  370.1 39.5 all-gather.24
  411.9 40.1 all-gather.26
  456.7 19.4 reduce-scatter.1
